TPU v7x, 32 devices: a whole 2x2x4 slice. The times are simulated.
32 devices in a mesh: sp: 8 (over z, y), tp: 4 (over x, core).
Axes of the slice: x: 2, y: 2, z: 4, core: 2. Of those that a mesh axis runs over, the one named last changes fastest.
Arguments:
- tokens: bfloat16 [4096, 2048], P(('sp', 'tp')), may hold values from -6 to 6
- queries: bfloat16 [4096, 1024], P('sp', 'tp'), may hold values from -160 to 160
- keys: bfloat16 [4096, 1024], P('sp', 'tp'), may hold values from -8 to 8
- values: bfloat16 [4096, 1024], P('sp', 'tp'), may hold values from -6 to 6
- lambdas: float32 [8], P('tp'), may hold values from 0.3 to 0.8
- head_gain: float32 [128], replicated, may hold values from 0.1 to 1.9
- out_weight: bfloat16 [1024, 2048], replicated, may hold values from -0.1875 to 0.1875
- mixer_gain: float32 [2048], replicated, may hold values from 0.1 to 1.9
- up_weight: bfloat16 [2048, 4096], P('sp', 'tp'), may hold values from -0.125 to 0.125
- down_weight: bfloat16 [4096, 2048], P('tp', 'sp'), may hold values from -0.09375 to 0.09375
Outputs:
- result: bfloat16 [4096, 2048], P(('sp', 'tp'))
All inputs are finite; a program needn't handle non-finite values.
Results may differ from a plain program's by a relative error of at most 0.02.
Values may be sent and summed in bfloat16 or wider, within the bound.
A program may use at most 128 MiB of HBM per device.

v0:
```python
import math
import jax
import jax.numpy as jnp
from jax import lax
from jax.sharding import PartitionSpec as P

DQK = 64
DV = 128


def per_device(
    tokens,
    queries,
    keys,
    values,
    lambdas,
    head_gain,
    out_weight,
    mixer_gain,
    up_weight,
    down_weight,
):
    tok_rows = queries.shape[0]
    head_count = lambdas.shape[0]
    scaling = DQK ** (-0.5)
    sp_index = lax.axis_index("sp")
    first_row = sp_index * tok_rows
    last_row = first_row + tok_rows - 1
    query_split = queries.reshape(tok_rows, head_count, 2, DQK)
    query_pos = first_row + lax.broadcasted_iota(jnp.int32, (tok_rows, 1), 0)
    floor_max = jnp.full((head_count, tok_rows), -1e30, jnp.float32)
    zero_total = jnp.zeros((head_count, tok_rows), jnp.float32)
    zero_acc = jnp.zeros((head_count, tok_rows, DV), jnp.float32)
    start_state = (floor_max, zero_total, zero_acc, floor_max, zero_total, zero_acc)
    key_piece = lax.all_gather(keys, "sp", axis=0, tiled=True)
    value_piece = lax.all_gather(values, "sp", axis=0, tiled=True)
    piece_rows = key_piece.shape[0]
    block_width = math.gcd(piece_rows, 512)

    def one_block(block_index, running):
        offset = block_index * block_width

        def update(inner):
            key_block = lax.dynamic_slice_in_dim(key_piece, offset, block_width, 0).reshape(
                block_width, head_count, 2, DQK
            )
            value_block = lax.dynamic_slice_in_dim(value_piece, offset, block_width, 0).reshape(
                block_width, head_count, DV
            )
            key_pos = offset + lax.broadcasted_iota(jnp.int32, (1, block_width), 1)
            allowed = key_pos <= query_pos
            updated = []
            for map_index in range(2):
                run_max = inner[3 * map_index]
                run_total = inner[3 * map_index + 1]
                run_acc = inner[3 * map_index + 2]
                scores = (
                    jnp.einsum(
                        "qhd,khd->hqk",
                        query_split[:, :, map_index],
                        key_block[:, :, map_index],
                        preferred_element_type=jnp.float32,
                    )
                    * scaling
                )
                scores = jnp.where(allowed[None], scores, -jnp.inf)
                new_max = jnp.maximum(run_max, jnp.max(scores, axis=2))
                shrink = jnp.exp(run_max - new_max)
                exponent = jnp.exp(scores - new_max[:, :, None])
                new_total = run_total * shrink + jnp.sum(exponent, axis=2)
                new_acc = run_acc * shrink[:, :, None] + jnp.einsum(
                    "hqk,khd->hqd",
                    exponent.astype(jnp.bfloat16),
                    value_block,
                    preferred_element_type=jnp.float32,
                )
                updated += [new_max, new_total, new_acc]
            return tuple(updated)

        return lax.cond(offset <= last_row, update, lambda inner: inner, running)

    final = lax.fori_loop(0, piece_rows // block_width, one_block, start_state)
    first_map = final[2] / final[1][:, :, None]
    second_map = final[5] / final[4][:, :, None]
    differ = first_map - lambdas[:, None, None] * second_map
    spread = lax.rsqrt(jnp.mean(differ * differ, axis=2, keepdims=True) + 1e-06)
    attended = (differ * spread * head_gain).astype(jnp.bfloat16)
    attended = jnp.transpose(attended, (1, 0, 2)).reshape(tok_rows, head_count * DV)
    all_heads = lax.all_to_all(attended, "tp", split_axis=0, concat_axis=1, tiled=True)
    projected = jnp.dot(all_heads, out_weight, preferred_element_type=jnp.float32).astype(
        jnp.bfloat16
    )
    resid = (tokens.astype(jnp.float32) + projected.astype(jnp.float32)).astype(jnp.bfloat16)
    resid_full = resid.astype(jnp.float32)
    normed = (
        resid_full
        * lax.rsqrt(jnp.mean(resid_full * resid_full, axis=1, keepdims=True) + 1e-06)
        * mixer_gain
    ).astype(jnp.bfloat16)
    up_full, down_full = (
        lax.all_gather(up_weight, "sp", axis=0, tiled=True),
        lax.all_gather(down_weight, "sp", axis=1, tiled=True),
    )
    hidden = jnp.square(
        jax.nn.relu(
            jnp.dot(
                lax.all_gather(normed, "tp", axis=0, tiled=True),
                up_full,
                preferred_element_type=jnp.float32,
            )
        )
    ).astype(jnp.bfloat16)
    mixed = lax.psum_scatter(
        jnp.dot(hidden, down_full, preferred_element_type=jnp.float32).astype(jnp.bfloat16),
        "tp",
        scatter_dimension=0,
        tiled=True,
    ).astype(jnp.float32)
    return (resid_full + mixed).astype(jnp.bfloat16)


def solution(mesh):
    placed = (
        P(("sp", "tp"), None),
        P("sp", "tp"),
        P("sp", "tp"),
        P("sp", "tp"),
        P("tp"),
        P(),
        P(),
        P(),
        P("sp", "tp"),
        P("tp", "sp"),
    )
    return jax.shard_map(
        per_device, mesh=mesh, in_specs=placed, out_specs=P(("sp", "tp"), None), check_vma=False
    )
```

profile of v0, /device:TPU:0, one launch (start us, length us, event | category | flops | bytes accessed | tf_op | source)
XLA Modules:
  0.0 390.4 jit_solution(7003081648482967234)
XLA Ops:
  6.5 0.0 all-gather.6.cloned.1.call-start
  6.5 1.8 copy.19
  8.3 0.0 all-gather.6.cloned.1.call-update
  8.4 0.0 all-gather.8.cloned.1.call-start
  8.4 1.8 copy.21
  10.2 0.0 all-gather.8.cloned.1.call-update
  10.2 0.0 all-gather.10.cloned.1.call-start
  10.3 1.1 copy.20
  11.4 51.1 %all-gather.6.cloned.1.call-done = bf16[4096,256]{0,1:T(8,128)(2,1)} async-done(((bf16[512,256]{0,1:T(8,128)(2,1)}), bf16[4096,256]{0,1:T(8,128)(2,1)}) %all-gather.6.cloned.1.call-update) | async-done | bytes 2097168 | tf_op jit(solution)/shard_map/all_gather | solution.py:35
  62.5 50.6 %all-gather.8.cloned.1.call-done = bf16[4096,256]{0,1:T(8,128)(2,1)} async-done(((bf16[512,256]{0,1:T(8,128)(2,1)}), bf16[4096,256]{0,1:T(8,128)(2,1)}) %all-gather.8.cloned.1.call-update) | async-done | bytes 2097168 | tf_op jit(solution)/shard_map/all_gather | solution.py:36
  113.2 0.0 copy-start.2
  113.2 0.0 copy-start.3
  113.2 6.1 %while.24 = (s32[]{:T(128)}, f32[2,512]{1,0:T(2,128)S(1)}, f32[2,512]{1,0:T(2,128)S(1)}, f32[2,512,128]{2,1,0:T(8,128)S(1)}, f32[2,512]{1,0:T(2,128)S(1)}, /*ind...) while((s32[]{:T(128)}, f32[2,512]{1,0:T(2,128)S(1)}, ...), condition=%wide.region_7.8_spmd.clone, body=%wide.region_0.7_spmd.clone.sunk | while | flops 410784768 | bytes 17707416 | solution.py:82
  113.3 5.6 %conditional.3 = ((f32[2,512]{1,0:T(2,128)S(1)}, f32[2,512]{1,0:T(2,128)S(1)}, f32[2,512,128]{2,1,0:T(8,128)S(1)}, f32[2,512]{1,0:T(2,128)S(1)}, f32[2,512]{1,0:T(2,128)S(1)}, /*index=5*/f32[2,512,128]{2,1,0:T(8,128)S(1)})) conditional(s32[]{:T(128)} %convert_element_type.94, (f32[2,512]{1,0:T(2,128)S(1)}, f32[2,512]{1,0:T(2,128)S(1)}, ...), branch_computations={%region_1.0_spmd, %region_2.6_spmd} | conditional | flops 410784768 | bytes 17705066 | solution.py:80
  113.3 1.0 constant_dynamic-slice_fusion.1
  114.3 0.2 broadcast_compare_fusion
  114.5 0.6 fusion.20
  115.2 0.3 fusion.3
  115.5 0.6 fusion.21
  116.1 0.3 fusion.5
  116.4 1.0 constant_dynamic-slice_fusion
  117.4 0.7 convolution_add_fusion
  118.1 0.7 convolution_add_fusion.1
  119.3 0.0 copy-done.2
  119.3 0.0 copy-start
  119.3 0.5 multiply_reduce_fusion.1
  119.9 0.0 copy-done.3
  119.9 0.2 fusion.18
  120.1 0.3 copy.23
  120.4 0.2 all_to_all.14
  120.5 8.5 %all_to_all.19 = bf16[4,128,256]{2,1,0:T(8,128)(2,1)S(1)} all-to-all(bf16[4,128,256]{2,1,0:T(8,128)(2,1)S(1)} %all_to_all.14), channel_id=1, replica_groups=mesh['sp'=8,'tp'=4] {'tp'}, dimensions={0} | all-to-all | bytes 524288 | tf_op jit(solution)/shard_map/all_to_all | solution.py:89
  129.1 0.2 copy.24
  129.3 0.0 copy-done
  129.3 0.0 copy-start.1
  129.3 3.0 multiply_reduce_fusion
  132.3 0.0 copy-done.1
  132.3 1.0 multiply_convert_fusion.1
  133.3 0.0 all-gather.10.cloned.1.call-update
  133.3 0.0 all-gather.12.cloned.1.call-start
  133.3 0.5 all-gather.12.cloned.1.call-update
  133.9 0.0 all-gather.14.cloned.1.call-start
  133.9 0.5 all-gather.14.cloned.1.call-update
  134.5 0.0 reduce-scatter.2.cloned.1.call-start
  134.5 57.8 %all-gather.10.cloned.1.call-done = bf16[512,2048]{1,0:T(8,128)(2,1)} async-done(((bf16[128,2048]{1,0:T(8,128)(2,1)}), bf16[512,2048]{1,0:T(8,128)(2,1)}) %all-gather.10.cloned.1.call-update) | async-done | bytes 2097168 | tf_op jit(solution)/shard_map/all_gather | solution.py:107
  192.3 74.8 %all-gather.12.cloned.1.call-done = bf16[2048,1024]{1,0:T(8,128)(2,1)} async-done(((bf16[256,1024]{1,0:T(8,128)(2,1)}), bf16[2048,1024]{1,0:T(8,128)(2,1)}) %all-gather.12.cloned.1.call-update) | async-done | bytes 4194320 | tf_op jit(solution)/shard_map/all_gather | solution.py:101
  267.1 75.1 %all-gather.14.cloned.1.call-done = bf16[1024,2048]{1,0:T(8,128)(2,1)} async-done(((bf16[1024,256]{1,0:T(8,128)(2,1)}), bf16[1024,2048]{1,0:T(8,128)(2,1)}) %all-gather.14.cloned.1.call-update) | async-done | bytes 4194320 | tf_op jit(solution)/shard_map/all_gather | solution.py:102
  342.2 9.9 %convolution_convert_fusion = bf16[512,2048]{1,0:T(8,128)(2,1)} fusion(bf16[1024,2048]{1,0:T(8,128)(2,1)} %all-gather.14.cloned.1.call-done, bf16[512,2048]{1,0:T(8,128)(2,1)} %all-gather.10.cloned.1.call-done, bf16[2048,1024]{1,0:T(8,128)(2,1)} %all-gather.12.cloned.1.call-done), kind=kOutput, calls=%fused_computation.28 | convolution fusion | flops 4297588736 | bytes 12582912 | tf_op jit(solution)/shard_map/dot_general | solution.py:114
  352.1 0.0 reduce-scatter.2.cloned.1.call-update
  352.1 29.5 %reduce-scatter.2.cloned.1.call-done = bf16[128,2048]{1,0:T(8,128)(2,1)} async-done(((bf16[512,2048]{1,0:T(8,128)(2,1)}), bf16[128,2048]{1,0:T(8,128)(2,1)}) %reduce-scatter.2.cloned.1.call-update) | async-done | bytes 524304 | tf_op jit(solution)/shard_map/reduce_scatter | solution.py:113
  381.6 1.9 add_convert_fusion
  (31 shorter events, 0.3 us)
Async XLA Ops:
  6.5 55.9 %all-gather.6.cloned.1.call-start = ((), (), s32[]{:S(2)}) async-start(), calls=%async_computation.2 | async-start | bytes 2359296 | tf_op jit(solution)/shard_map/all_gather | solution.py:35
  8.4 104.7 %all-gather.8.cloned.1.call-start = ((), (), s32[]{:S(2)}) async-start(), calls=%async_computation.3 | async-start | bytes 2359296 | tf_op jit(solution)/shard_map/all_gather | solution.py:36
  10.2 182.1 %all-gather.10.cloned.1.call-start = ((), (), s32[]{:S(2)}) async-start(), calls=%async_computation.4 | async-start | bytes 2621440 | tf_op jit(solution)/shard_map/all_gather | solution.py:107
  113.2 6.1 %copy-start.2 = (f32[2]{0:T(128)S(1)}, f32[2]{0:T(128)}, u32[]{:S(2)}) copy-start(f32[2]{0:T(128)} %param.18) | copy-start | bytes 28
  113.2 6.6 %copy-start.3 = (f32[128]{0:T(128)S(1)}, f32[128]{0:T(128)}, u32[]{:S(2)}) copy-start(f32[128]{0:T(128)} %param.19) | copy-start | bytes 1540
  119.3 9.9 %copy-start = (bf16[128,2048]{1,0:T(8,128)(2,1)S(1)}, bf16[128,2048]{1,0:T(8,128)(2,1)}, u32[]{:S(2)}) copy-start(bf16[128,2048]{1,0:T(8,128)(2,1)} %param.14) | copy-start | bytes 1572868
  129.3 3.0 copy-start.1
  133.3 133.8 %all-gather.12.cloned.1.call-start = ((), (), s32[]{:S(2)}) async-start(), calls=%async_computation.5 | async-start | bytes 4718592 | tf_op jit(solution)/shard_map/all_gather | solution.py:101
  133.9 208.3 %all-gather.14.cloned.1.call-start = ((), (), s32[]{:S(2)}) async-start(), calls=%async_computation.6 | async-start | bytes 4718592 | tf_op jit(solution)/shard_map/all_gather | solution.py:102
  134.5 247.2 %reduce-scatter.2.cloned.1.call-start = ((), (), s32[]{:S(2)}) async-start(), calls=%async_computation.7 | async-start | bytes 2621440 | tf_op jit(solution)/shard_map/reduce_scatter | solution.py:113
Sparse Core Ops, SparseCore 0:
  9.4 53.0 all-gather.5
  64.5 48.5 all-gather.7
  133.4 58.8 all-gather.9
  194.3 72.7 all-gather.11
  269.0 73.1 all-gather.13
  352.3 29.3 reduce-scatter.1
where the time goes:
time: 391 us; the launch traced here: 390 us
  waiting for transfers between devices  340 us (87%)
  matrix products  15.6 us (4%)
  between operations  13.6 us (3%)
  blocking collectives  8.55 us (2%)
  local copies, waits for them, and re-layouts  7.41 us (2%)
  other arithmetic  4.49 us (1%)
    all_gather x1, waiting for transfers between devices, per_device(): lax.all_gather(down_weight, 'sp', axis=1, tiled=True)  75.1 us
    all_gather x1, waiting for transfers between devices, per_device(): lax.all_gather(up_weight, 'sp', axis=0, tiled=True)  74.8 us
    all_gather x1, waiting for transfers between devices, per_device(): lax.all_gather(normed, 'tp', axis=0, tiled=True)  57.8 us
    all_gather x1, waiting for transfers between devices, per_device(): key_piece = lax.all_gather(keys, 'sp', axis=0, tiled=True)  51.1 us
    all_gather x1, waiting for transfers between devices, per_device(): value_piece = lax.all_gather(values, 'sp', axis=0, tiled=True)  50.6 us
    reduce_scatter x1, waiting for transfers between devices, per_device(): lax.psum_scatter(jnp.dot(hidden, down_full, preferred_element_type=jnp.fl...  29.5 us
    dot_general x1, matrix products, per_device(): jnp.dot(hidden, down_full, preferred_element_type=jnp.float32)  9.93 us
    all_to_all x1, blocking collectives, per_device(): lax.all_to_all(attended, 'tp', split_axis=0, concat_axis=1, tiled=True)  8.55 us
  transfers between devices with their start and end apart: 6, of which 6 were waited for; matrix products, arithmetic and copies ran while one was open for 1% of the time, Pallas kernels for 0%

commit v1 on v0

--- a/solution.py
+++ b/solution.py
@@ -99,7 +99,7 @@
     ).astype(jnp.bfloat16)
     up_full, down_full = (
         lax.all_gather(up_weight, "sp", axis=0, tiled=True),
-        lax.all_gather(down_weight, "sp", axis=1, tiled=True),
+        jnp.concatenate(lax.all_gather(down_weight, "sp"), axis=1),
     )
     hidden = jnp.square(
         jax.nn.relu(

time: 391 us -> 333 us (0.85)
  waiting for transfers between devices: 340 us -> 276 us
  local copies, waits for them, and re-layouts: 7.41 us -> 13 us
    all_gather x1, waiting for transfers between devices: 57.8 us -> 16.1 us  [per_device(): lax.all_gather(normed, 'tp', axis=0, tiled=True)]
    all_gather x1, waiting for transfers between devices: 75.1 us -> 52.3 us  [per_device(): lax.all_gather(down_weight, 'sp')]
    reshape x0 -> x1, local copies, waits for them, and re-layouts: none -> 6.47 us  [per_device(): jnp.concatenate(lax.all_gather(down_weight, 'sp'), axis=1)]
  transfers between devices with their start and end apart: 6 -> 6, of which waited for: 6 -> 6; matrix products, arithmetic and copies ran while one was open for 1% -> 6% of each run, Pallas kernels for 0% -> 0%
where the time goes in v1:
time: 333 us; the launch traced here: 332 us
  waiting for transfers between devices  276 us (83%)
  matrix products  15.6 us (5%)
  between operations  13.7 us (4%)
  local copies, waits for them, and re-layouts  13 us (4%)
  blocking collectives  8.55 us (3%)
  other arithmetic  4.49 us (1%)
    all_gather x1, waiting for transfers between devices, per_device(): lax.all_gather(up_weight, 'sp', axis=0, tiled=True)  74.8 us
    all_gather x1, waiting for transfers between devices, per_device(): lax.all_gather(down_weight, 'sp')  52.3 us
    all_gather x1, waiting for transfers between devices, per_device(): key_piece = lax.all_gather(keys, 'sp', axis=0, tiled=True)  51.2 us
    all_gather x1, waiting for transfers between devices, per_device(): value_piece = lax.all_gather(values, 'sp', axis=0, tiled=True)  50.6 us
    reduce_scatter x1, waiting for transfers between devices, per_device(): lax.psum_scatter(jnp.dot(hidden, down_full, preferred_element_type=jnp.fl...  29.8 us
    all_gather x1, waiting for transfers between devices, per_device(): lax.all_gather(normed, 'tp', axis=0, tiled=True)  16.1 us
    dot_general x1, matrix products, per_device(): jnp.dot(hidden, down_full, preferred_element_type=jnp.float32)  9.9 us
    all_to_all x1, blocking collectives, per_device(): lax.all_to_all(attended, 'tp', split_axis=0, concat_axis=1, tiled=True)  8.55 us
  transfers between devices with their start and end apart: 6, of which 6 were waited for; matrix products, arithmetic and copies ran while one was open for 6% of the time, Pallas kernels for 0%

profile of v1, /device:TPU:0, one launch (start us, length us, event | category | flops | bytes accessed | tf_op | source)
XLA Modules:
  0.0 332.2 jit_solution(3469055220679544376)
XLA Ops:
  6.5 0.0 copy-start.1
  6.5 0.0 all-gather.7.cloned.1.call-start
  6.5 1.8 copy.31
  8.4 0.0 all-gather.7.cloned.1.call-update
  8.4 0.0 all-gather.9.cloned.1.call-start
  8.5 1.8 copy.33
  10.3 0.0 all-gather.9.cloned.1.call-update
  10.3 0.0 all-gather.15.cloned.1.call-start
  10.3 0.7 all-gather.15.cloned.1.call-update
  11.0 0.0 all-gather.11.cloned.1.call-start
  11.1 0.0 copy-done.1
  11.1 0.1 copy.32
  11.3 51.2 %all-gather.7.cloned.1.call-done = bf16[4096,256]{0,1:T(8,128)(2,1)} async-done(((bf16[512,256]{0,1:T(8,128)(2,1)}), bf16[4096,256]{0,1:T(8,128)(2,1)}) %all-gather.7.cloned.1.call-update) | async-done | bytes 2097168 | tf_op jit(solution)/shard_map/all_gather | solution.py:35
  62.5 50.6 %all-gather.9.cloned.1.call-done = bf16[4096,256]{0,1:T(8,128)(2,1)} async-done(((bf16[512,256]{0,1:T(8,128)(2,1)}), bf16[4096,256]{0,1:T(8,128)(2,1)}) %all-gather.9.cloned.1.call-update) | async-done | bytes 2097168 | tf_op jit(solution)/shard_map/all_gather | solution.py:36
  113.2 0.0 copy-start.3
  113.2 0.0 copy-start.4
  113.2 6.1 %while.24 = (s32[]{:T(128)}, f32[2,512]{1,0:T(2,128)S(1)}, f32[2,512]{1,0:T(2,128)S(1)}, f32[2,512,128]{2,1,0:T(8,128)S(1)}, f32[2,512]{1,0:T(2,128)S(1)}, /*ind...) while((s32[]{:T(128)}, f32[2,512]{1,0:T(2,128)S(1)}, ...), condition=%wide.region_7.8_spmd.clone, body=%wide.region_0.7_spmd.clone.sunk | while | flops 410784768 | bytes 17707416 | solution.py:82
  113.3 5.6 %conditional.3 = ((f32[2,512]{1,0:T(2,128)S(1)}, f32[2,512]{1,0:T(2,128)S(1)}, f32[2,512,128]{2,1,0:T(8,128)S(1)}, f32[2,512]{1,0:T(2,128)S(1)}, f32[2,512]{1,0:T(2,128)S(1)}, /*index=5*/f32[2,512,128]{2,1,0:T(8,128)S(1)})) conditional(s32[]{:T(128)} %convert_element_type.94, (f32[2,512]{1,0:T(2,128)S(1)}, f32[2,512]{1,0:T(2,128)S(1)}, ...), branch_computations={%region_1.0_spmd, %region_2.6_spmd} | conditional | flops 410784768 | bytes 17705066 | solution.py:80
  113.3 1.0 constant_dynamic-slice_fusion.1
  114.3 0.2 broadcast_compare_fusion
  114.5 0.6 fusion.20
  115.2 0.3 fusion.3
  115.5 0.6 fusion.21
  116.1 0.3 fusion.5
  116.4 1.0 constant_dynamic-slice_fusion
  117.4 0.7 convolution_add_fusion
  118.1 0.7 convolution_add_fusion.1
  119.3 0.0 copy-done.3
  119.3 0.0 copy-start
  119.3 0.5 multiply_reduce_fusion.1
  119.8 0.0 copy-done.4
  119.8 0.2 fusion.18
  120.1 0.3 copy.35
  120.3 0.2 all_to_all.14
  120.5 8.5 %all_to_all.19 = bf16[4,128,256]{2,1,0:T(8,128)(2,1)S(1)} all-to-all(bf16[4,128,256]{2,1,0:T(8,128)(2,1)S(1)} %all_to_all.14), channel_id=1, replica_groups=mesh['sp'=8,'tp'=4] {'tp'}, dimensions={0} | all-to-all | bytes 524288 | tf_op jit(solution)/shard_map/all_to_all | solution.py:89
  129.1 0.2 copy.36
  129.2 0.0 copy-done
  129.2 0.0 copy-start.2
  129.3 3.0 multiply_reduce_fusion
  132.3 0.0 copy-done.2
  132.3 1.0 multiply_convert_fusion.1
  133.3 0.0 all-gather.11.cloned.1.call-update
  133.3 0.0 all-gather.13.cloned.1.call-start
  133.3 0.5 all-gather.13.cloned.1.call-update
  133.9 0.0 reduce-scatter.2.cloned.1.call-start
  133.9 52.3 %all-gather.15.cloned.1.call-done = bf16[8192,256]{1,0:T(8,128)(2,1)} async-done(((bf16[1024,256]{1,0:T(8,128)(2,1)}), bf16[8192,256]{1,0:T(8,128)(2,1)}) %all-gather.15.cloned.1.call-update) | async-done | bytes 4194320 | tf_op jit(solution)/shard_map/all_gather | solution.py:102
  186.2 6.5 %copy.37 = bf16[1024,8,256]{0,2,1:T(8,128)(2,1)} copy(bf16[1024,8,256]{2,0,1:T(8,128)(2,1)} %bitcast.51) | data formatting | bytes 8388608 | tf_op jit(solution)/shard_map/reshape | solution.py:102
  192.7 16.1 %all-gather.11.cloned.1.call-done = bf16[512,2048]{1,0:T(8,128)(2,1)} async-done(((bf16[128,2048]{1,0:T(8,128)(2,1)}), bf16[512,2048]{1,0:T(8,128)(2,1)}) %all-gather.11.cloned.1.call-update) | async-done | bytes 2097168 | tf_op jit(solution)/shard_map/all_gather | solution.py:107
  208.8 74.8 %all-gather.13.cloned.1.call-done = bf16[2048,1024]{1,0:T(8,128)(2,1)} async-done(((bf16[256,1024]{1,0:T(8,128)(2,1)}), bf16[2048,1024]{1,0:T(8,128)(2,1)}) %all-gather.13.cloned.1.call-update) | async-done | bytes 4194320 | tf_op jit(solution)/shard_map/all_gather | solution.py:101
  283.6 9.9 %convolution_convert_fusion = bf16[512,2048]{1,0:T(8,128)(2,1)} fusion(bf16[1024,2048]{0,1:T(8,128)(2,1)} %bitcast.52, bf16[512,2048]{1,0:T(8,128)(2,1)} %all-gather.11.cloned.1.call-done, bf16[2048,1024]{1,0:T(8,128)(2,1)} %all-gather.13.cloned.1.call-done), kind=kOutput, calls=%fused_computation.28 | convolution fusion | flops 4297588736 | bytes 12582912 | tf_op jit(solution)/shard_map/dot_general | solution.py:114
  293.5 0.0 reduce-scatter.2.cloned.1.call-update
  293.5 29.8 %reduce-scatter.2.cloned.1.call-done = bf16[128,2048]{1,0:T(8,128)(2,1)} async-done(((bf16[512,2048]{1,0:T(8,128)(2,1)}), bf16[128,2048]{1,0:T(8,128)(2,1)}) %reduce-scatter.2.cloned.1.call-update) | async-done | bytes 524304 | tf_op jit(solution)/shard_map/reduce_scatter | solution.py:113
  323.4 1.9 add_convert_fusion
  (31 shorter events, 0.3 us)
Async XLA Ops:
  6.5 4.6 %copy-start.1 = (bf16[512,256]{1,0:T(8,128)(2,1)S(1)}, bf16[512,256]{1,0:T(8,128)(2,1)}, u32[]{:S(2)}) copy-start(bf16[512,256]{1,0:T(8,128)(2,1)} %param.15) | copy-start | bytes 786436
  6.5 55.9 %all-gather.7.cloned.1.call-start = ((), (), s32[]{:S(2)}) async-start(), calls=%async_computation.2 | async-start | bytes 2359296 | tf_op jit(solution)/shard_map/all_gather | solution.py:35
  8.4 104.7 %all-gather.9.cloned.1.call-start = ((), (), s32[]{:S(2)}) async-start(), calls=%async_computation.3 | async-start | bytes 2359296 | tf_op jit(solution)/shard_map/all_gather | solution.py:36
  10.3 175.9 %all-gather.15.cloned.1.call-start = ((), (), s32[]{:S(2)}) async-start(), calls=%async_computation.7 | async-start | bytes 4718592 | tf_op jit(solution)/shard_map/all_gather | solution.py:102
  11.0 197.8 %all-gather.11.cloned.1.call-start = ((), (), s32[]{:S(2)}) async-start(), calls=%async_computation.4 | async-start | bytes 2621440 | tf_op jit(solution)/shard_map/all_gather | solution.py:107
  113.2 6.1 %copy-start.3 = (f32[2]{0:T(128)S(1)}, f32[2]{0:T(128)}, u32[]{:S(2)}) copy-start(f32[2]{0:T(128)} %param.18) | copy-start | bytes 28
  113.2 6.6 %copy-start.4 = (f32[128]{0:T(128)S(1)}, f32[128]{0:T(128)}, u32[]{:S(2)}) copy-start(f32[128]{0:T(128)} %param.19) | copy-start | bytes 1540
  119.3 9.9 %copy-start = (bf16[128,2048]{1,0:T(8,128)(2,1)S(1)}, bf16[128,2048]{1,0:T(8,128)(2,1)}, u32[]{:S(2)}) copy-start(bf16[128,2048]{1,0:T(8,128)(2,1)} %param.14) | copy-start | bytes 1572868
  129.2 3.1 copy-start.2
  133.3 150.3 %all-gather.13.cloned.1.call-start = ((), (), s32[]{:S(2)}) async-start(), calls=%async_computation.5 | async-start | bytes 4718592 | tf_op jit(solution)/shard_map/all_gather | solution.py:101
  133.9 189.5 %reduce-scatter.2.cloned.1.call-start = ((), (), s32[]{:S(2)}) async-start(), calls=%async_computation.6 | async-start | bytes 2621440 | tf_op jit(solution)/shard_map/reduce_scatter | solution.py:113
Sparse Core Ops, SparseCore 0:
  9.4 53.0 all-gather.6
  64.5 48.5 all-gather.8
  115.2 70.9 all-gather.14
  187.6 21.1 all-gather.10
  210.8 72.7 all-gather.12
  293.7 29.6 reduce-scatter.1
